TPU v7x, 32 devices: a whole 2x2x4 slice. The times are simulated.
32 devices in a mesh: grp: 2 (over y), sp: 4 (over z), dp: 4 (over x, core).
Axes of the slice: x: 2, y: 2, z: 4, core: 2. Of those that a mesh axis runs over, the one named last changes fastest.
Arguments:
- queries: bfloat16 [8, 512, 16, 192], P(('grp', 'dp'), 'sp'), parts along dimension 0, may hold values from -41 to 41
- kv_latent: bfloat16 [8, 512, 512], P(('grp', 'dp'), 'sp'), parts along dimension 0, may hold values from -6 to 6
- rope_key: bfloat16 [8, 512, 64], P(('grp', 'dp'), 'sp'), parts along dimension 0, may hold values from -5.1 to 5.1
- kv_gain: float32 [512], replicated, may hold values from 0.1 to 1.9
- kv_weight: bfloat16 [512, 4096], P('dp', 'sp'), may hold values from -0.25 to 0.25
- out_weight: bfloat16 [2048, 2048], P(None, 'dp'), may hold values from -1 to 1
Outputs:
- mixed: bfloat16 [8, 512, 2048], P(('grp', 'dp'), 'sp'), parts along dimension 0
There are 2 independent parts, one for each index of `grp`. A program takes and returns all parts, laid end to end along the dimension named above; an argument that names none is the same for every part. Nothing has to cross between parts.
All inputs are finite; a program needn't handle non-finite values.
Results may differ from a plain program's by a relative error of at most 0.0075.
Values may be sent and summed in bfloat16 or wider, within the bound.
A program may use at most 64 MiB of HBM per device.

v0:
```python
import functools
import math

import jax
import jax.numpy as jnp
import numpy as np
from jax import lax
from jax.experimental import pallas as pl
from jax.experimental.pallas import tpu as pltpu
from jax.sharding import PartitionSpec as P

NOPE = 128
VD = 128
LANES = 128
CORES = 2
CHUNKS = 8
LEAD = 3
MESH = pl.DeviceIdType.MESH


VARIANTS = 4


def rotation_table(length, rope):
    half = rope // 2
    inverse = np.power(10000.0, -np.arange(half) * 2.0 / rope).astype(np.float32)
    angle = inverse[:, None] * np.arange(length, dtype=np.float32)[None, :]
    return np.stack([np.cos(angle), np.sin(angle)]).astype(np.float32)


def kernel(
    n, g, nx, hn, rope, scale, chunks,
    q_ref, latent_ref, key_ref, gain_ref, table_ref, kvw_ref, w_ref, out_ref,
    qbuf, lat, kvw, wfull, kcat, vbuf, attsend, attrecv, acc,
    loc, q_s, q_r, a_s, a_r, lr_s, lr_r, rl_s, rl_r,
    kx_s, kx_r, kc_s, kc_r, wx_s, wx_r, wy_s, wy_r, wc_s, wc_r, wo_s, wo_r,
):
    me = lax.axis_index("sp")
    y = lax.axis_index("grp")
    dp = lax.axis_index("dp")
    x, c = dp // CORES, dp % CORES
    ndp = nx * CORES
    tok = latent_ref.shape[0]
    half = rope // 2
    lat_ref = lat.at[me]
    latw = kvw.shape[0]
    length = n * tok
    krows = kvw_ref.shape[0]
    part = w_ref.shape[0] // g
    crow = part // chunks
    cols = w_ref.shape[1]
    kd = hn * VD

    def xor(a, b):
        total, bit = 0, 1
        while bit < n:
            total = total + bit * lax.rem(lax.div(a, bit) + lax.div(jnp.int32(b), bit), 2)
            bit *= 2
        return total

    paired = n & (n - 1) == 0

    def target(o):
        return xor(me, o) if paired else lax.rem(me + o, n)

    def source(o):
        return xor(me, o) if paired else lax.rem(me + n - o, n)

    def turned(values, j):
        span = pl.ds(pl.multiple_of(j * tok, tok), tok)
        cosine, sine = table_ref[0, :, span], table_ref[1, :, span]
        first, second = values[:half].astype(jnp.float32), values[half:].astype(jnp.float32)
        return first * cosine - second * sine, first * sine + second * cosine

    def chip(xx, cc):
        return {"dp": xx * CORES + cc}

    partner = chip(x, 1 - c)

    def remote(src, dst, ss, rs, dev):
        return pltpu.make_async_remote_copy(
            src_ref=src, dst_ref=dst, send_sem=ss, recv_sem=rs, device_id=dev, device_id_type=MESH
        )

    own_w = pltpu.make_async_copy(w_ref, wfull.at[dp], loc.at[0])
    own_k = pltpu.make_async_copy(
        kvw_ref, kvw.at[pl.ds(pl.multiple_of(dp * krows, krows), krows)], loc.at[1]
    )
    own_q = pltpu.make_async_copy(q_ref.at[pl.ds(me * hn, hn)], qbuf.at[me], loc.at[2])
    for copy in (own_k, own_q, own_w):
        copy.start()

    barrier = pltpu.get_barrier_semaphore()
    for o in range(1, n):
        pl.semaphore_signal(barrier, 1, device_id={"sp": lax.rem(me + o, n)}, device_id_type=MESH)
    for o in range(1, nx):
        pl.semaphore_signal(barrier, 1, device_id=chip(lax.rem(x + o, nx), c), device_id_type=MESH)
    for o in range(1, g):
        pl.semaphore_signal(barrier, 1, device_id={"grp": lax.rem(y + o, g)}, device_id_type=MESH)
    pl.semaphore_signal(barrier, 1, device_id=partner, device_id_type=MESH)

    latent = latent_ref[...].astype(jnp.float32)
    square = jnp.mean(latent * latent, axis=-1, keepdims=True)
    lat[me, :, :latw] = (latent * lax.rsqrt(square + 1e-06) * gain_ref[...]).astype(jnp.bfloat16)
    first, second = turned(key_ref[...], me)
    rest = jnp.zeros((LANES - rope, tok), jnp.float32)
    lat[me, :, latw:] = jnp.concatenate([first, second, rest], axis=0).T.astype(jnp.bfloat16)

    pl.semaphore_wait(barrier, (n - 1) + (nx - 1) + (g - 1) + 1)

    def to_right(k, src):
        j = me - k
        return remote(src, lat.at[j], lr_s.at[k], lr_r.at[k], {"sp": me + 1})

    def to_left(k, src):
        j = me + k
        return remote(src, lat.at[j], rl_s.at[k], rl_r.at[k], {"sp": me - 1})

    @pl.when(me < n - 1)
    def _():
        to_right(0, lat_ref).start()

    @pl.when(me > 0)
    def _():
        to_left(0, lat_ref).start()

    def kv_rows(d):
        return kvw.at[pl.ds(pl.multiple_of(d * krows, krows), krows)]

    def kv_x(o):
        return remote(kvw_ref, kv_rows(dp), kx_s.at[o - 1], kx_r.at[o - 1], chip(lax.rem(x + o, nx), c))

    def kv_core(o):
        d = lax.rem(x + nx - o, nx) * CORES + c
        src = kvw_ref if o == 0 else kv_rows(d)
        return remote(src, kv_rows(d), kc_s.at[o], kc_r.at[o], partner)

    for o in range(1, nx):
        kv_x(o).start()
    kv_core(0).start()

    def q_copy(o):
        to = target(o)
        return remote(q_ref.at[pl.ds(to * hn, hn)], qbuf.at[me], q_s.at[o], q_r.at[o], {"sp": to})

    def w_rows(yy, ch):
        return pl.ds(pl.multiple_of(yy * part + ch * crow, crow), crow)

    def w_x(o, ch):
        rows = w_rows(y, ch)
        return remote(
            w_ref.at[rows], wfull.at[dp, rows], wx_s.at[o - 1, ch], wx_r.at[o - 1, ch],
            chip(lax.rem(x + o, nx), c),
        )

    def w_y(o, p, ch):
        ref = wfull.at[lax.rem(x + nx - o, nx) * CORES + c, w_rows(y, ch)]
        return remote(
            ref, ref, wy_s.at[o - 1, p - 1, ch], wy_r.at[o - 1, p - 1, ch],
            {"grp": lax.rem(y + p, g)},
        )

    def w_c(o, p, ch):
        ref = wfull.at[lax.rem(x + nx - o, nx) * CORES + c, w_rows(lax.rem(y + g - p, g), ch)]
        return remote(ref, ref, wc_s.at[o - 1, p, ch], wc_r.at[o - 1, p, ch], partner)

    w_own = remote(w_ref, wfull.at[dp], wo_s, wo_r, partner)
    w_own.start()

    def start_queries():
        for o in range(1, n):
            q_copy(o).start()

    def take_kv():
        for o in range(1, nx):
            kv_x(o).wait_recv()
            kv_core(o).start()
        for ch in range(min(LEAD, chunks)):
            for o in range(1, nx):
                w_x(o, ch).start()

    for k in range(1, n):
        @pl.when(me - k >= 0)
        def _():
            to_right(k - 1, lat_ref).wait_recv()

            @pl.when(me < n - 1)
            def _():
                to_right(k, lat.at[me - k]).start()

        @pl.when(me + k < n)
        def _():
            to_left(k - 1, lat_ref).wait_recv()

            @pl.when(me > 0)
            def _():
                to_left(k, lat.at[me + k]).start()

        if k == n - 1:
            start_queries()
        if k == 1:
            take_kv()

    own_k.wait()
    for o in range(nx):
        kv_core(o).wait_recv()

    @pl.loop(0, n)
    def _(j):
        rows = pl.ds(pl.multiple_of(j * tok, tok), tok)
        block = lat[j, :, :latw]
        shared = lat[j, :, latw:]
        for h in range(hn):
            wide = NOPE + VD
            both = jnp.dot(
                block, kvw[:, h * wide : (h + 1) * wide], preferred_element_type=jnp.float32
            )
            kcat[h, rows, :NOPE] = both[:, :NOPE].astype(jnp.bfloat16)
            kcat[h, rows, NOPE:] = shared
            vbuf[h, :, rows] = both[:, NOPE:].T.astype(jnp.bfloat16)

    def pass_x(ch):
        for o in range(1, nx):
            w_x(o, ch).wait_recv()

            @pl.when(ch + LEAD < chunks)
            def _():
                w_x(o, ch + LEAD).start()

            for p in range(1, g):
                w_y(o, p, ch).start()
            w_c(o, 0, ch).start()

    def pass_y(ch):
        for o in range(1, nx):
            for p in range(1, g):
                w_y(o, p, ch).wait_recv()
                w_c(o, p, ch).start()

    variants = math.gcd(VARIANTS, n)
    step = length // variants

    def attention_over(j, extent):
        row = lax.broadcasted_iota(jnp.int32, (step, tok), 0)
        col = lax.broadcasted_iota(jnp.int32, (step, tok), 1)
        kept = row - col <= j * tok - (extent - step)
        pad = jnp.zeros((LANES - rope, tok), jnp.bfloat16)
        for h in range(hn):
            first, second = turned(qbuf[j, h, NOPE:, :], j)
            query = jnp.concatenate(
                [qbuf[j, h, :NOPE, :], first.astype(jnp.bfloat16), second.astype(jnp.bfloat16), pad],
                axis=0,
            )
            s = jnp.dot(kcat[h, :extent, :], query, preferred_element_type=jnp.float32)
            last = jnp.where(kept, s[extent - step :], -jnp.inf)
            s = last if extent == step else jnp.concatenate([s[: extent - step], last], axis=0)
            top = jnp.max(s, axis=0, keepdims=True)
            e = jnp.exp2((s - top) * (scale * math.log2(math.e)))
            p = (e * (1.0 / jnp.sum(e, axis=0, keepdims=True))).astype(jnp.bfloat16)
            o = jnp.dot(vbuf[h, :, :extent], p, preferred_element_type=jnp.float32)
            attsend[j, :, h * VD : (h + 1) * VD] = o.T.astype(jnp.bfloat16)

    def attention(j):
        for v in range(variants):
            @pl.when(j // (n // variants) == v)
            def _():
                attention_over(j, (v + 1) * step)

    def a_copy(o):
        to = source(o)
        return remote(attsend.at[to], attrecv.at[me], a_s.at[o], a_r.at[o], {"sp": to})

    own_q.wait()
    per = -(-chunks // n)
    for b in range(min(per, chunks)):
        pass_x(b)

    @pl.loop(0, n)
    def _(o):
        @pl.when(o > 0)
        def _():
            q_copy(o).wait_recv()

        attention(source(o))

        @pl.when(o > 0)
        def _():
            a_copy(o).start()

        for b in range(per):
            @pl.when((o + 1) * per + b < chunks)
            def _():
                pass_x((o + 1) * per + b)

            @pl.when(o * per + b < chunks)
            def _():
                pass_y(o * per + b)

    own_w.wait()
    w_own.wait_recv()
    for o in range(1, nx):
        for p in range(g):
            for ch in range(chunks):
                w_c(o, p, ch).wait_recv()

    def project(j, first):
        rows = pl.ds(pl.multiple_of(j * kd, kd), kd)
        block = attsend[me] if first else attrecv[j]
        for d in range(ndp):
            part_sum = jnp.dot(block, wfull[d, rows, :], preferred_element_type=jnp.float32)
            if first:
                acc[:, d * cols : (d + 1) * cols] = part_sum
            else:
                acc[:, d * cols : (d + 1) * cols] += part_sum

    project(me, True)

    @pl.loop(1, n)
    def _(o):
        a_copy(o).wait_recv()
        project(target(o), False)

    out_ref[...] = acc[...].astype(out_ref.dtype)

    for k in range(n - 1):
        @pl.when((me - k >= 0) & (me < n - 1))
        def _():
            to_right(k, lat_ref).wait_send()

        @pl.when((me + k < n) & (me > 0))
        def _():
            to_left(k, lat_ref).wait_send()
    for o in range(1, n):
        q_copy(o).wait_send()
        a_copy(o).wait_send()
    w_own.wait_send()
    for o in range(nx):
        kv_core(o).wait_send()
    for o in range(1, nx):
        kv_x(o).wait_send()
        for ch in range(chunks):
            w_x(o, ch).wait_send()
            for p in range(1, g):
                w_y(o, p, ch).wait_send()
            for p in range(g):
                w_c(o, p, ch).wait_send()


def body(sizes, queries, kv_latent, rope_key, kv_gain, kv_weight, out_weight):
    g, n, dp = sizes
    nx = dp // CORES
    tok, heads, width = queries.shape[1:]
    rope = width - NOPE
    hn = heads // n
    latw = kv_latent.shape[2]
    q = jnp.transpose(queries[0], (1, 2, 0))
    key = jnp.transpose(rope_key[0])
    table = jnp.asarray(rotation_table(n * tok, rope))

    d_in, cols = out_weight.shape
    part = d_in // g
    chunks = CHUNKS
    kcols = kv_weight.shape[1]
    dma = pltpu.SemaphoreType.DMA
    bf = jnp.bfloat16
    xn = max(nx - 1, 1)
    gn = max(g - 1, 1)
    vmem = pl.BlockSpec(memory_space=pltpu.VMEM)
    hbm = pl.BlockSpec(memory_space=pltpu.HBM)
    out = pl.pallas_call(
        functools.partial(kernel, n, g, nx, hn, rope, width**-0.5, chunks),
        out_shape=jax.ShapeDtypeStruct((tok, cols * dp), bf),
        in_specs=[hbm, vmem, vmem, vmem, vmem, hbm, hbm],
        out_specs=vmem,
        scratch_shapes=[
            pltpu.VMEM((n, hn, width, tok), bf),
            pltpu.VMEM((n, tok, latw + LANES), bf),
            pltpu.VMEM((kv_weight.shape[0] * dp, kcols), bf),
            pltpu.VMEM((dp, d_in, cols), bf),
            pltpu.VMEM((hn, n * tok, NOPE + LANES), bf),
            pltpu.VMEM((hn, VD, n * tok), bf),
            pltpu.VMEM((n, tok, hn * VD), bf),
            pltpu.VMEM((n, tok, hn * VD), bf),
            pltpu.VMEM((tok, cols * dp), jnp.float32),
            dma((3,)),
            dma((n,)), dma((n,)), dma((n,)), dma((n,)),
            dma((n,)), dma((n,)), dma((n,)), dma((n,)),
            dma((xn,)), dma((xn,)), dma((nx,)), dma((nx,)),
            dma((xn, chunks)), dma((xn, chunks)),
            dma((xn, gn, chunks)), dma((xn, gn, chunks)),
            dma((xn, g, chunks)), dma((xn, g, chunks)),
            dma(()), dma(()),
        ],
        compiler_params=pltpu.CompilerParams(
            collective_id=0, has_side_effects=True, vmem_limit_bytes=28 * 1024 * 1024
        ),
    )(q, kv_latent[0], key, kv_gain[None], table, kv_weight, out_weight)
    return out[None]


def solution(mesh):
    sizes = (mesh.shape["grp"], mesh.shape["sp"], mesh.shape["dp"])
    return jax.shard_map(
        functools.partial(body, sizes),
        mesh=mesh,
        in_specs=(
            P(("grp", "dp"), "sp", None, None),
            P(("grp", "dp"), "sp", None),
            P(("grp", "dp"), "sp", None),
            P(),
            P("dp", "sp"),
            P(None, "dp"),
        ),
        out_specs=P(("grp", "dp"), "sp", None),
        check_vma=False,
    )
```

profile of v0, /device:TPU:0, one launch (start us, length us, event | category | flops | bytes accessed | tf_op | source)
XLA Modules:
  0.0 59.6 jit_solution(8873120649703272149)
XLA Ops:
  0.0 0.0 copy-start
  0.0 1.6 %copy-done = bf16[2048,512]{1,0:T(8,128)(2,1)S(1)} copy-done((bf16[2048,512]{1,0:T(8,128)(2,1)S(1)}, bf16[2048,512]{1,0:T(8,128)(2,1)}, u32[]{:S(2)}) %copy-start) | copy-done | bytes 2097176
  1.6 0.0 copy-start.1
  1.6 1.1 %copy-done.1 = bf16[1,128,16,192]{1,3,2,0:T(8,128)(2,1)S(1)} copy-done((bf16[1,128,16,192]{1,3,2,0:T(8,128)(2,1)S(1)}, bf16[1,128,16,192]{1,3,2,0:T(8,128)(2,1)}, u32[]{:S(2)}) %copy-start.1) | copy-done | bytes 786456
  2.7 0.0 copy-start.2
  2.7 0.9 %copy-done.2 = bf16[128,1024]{1,0:T(8,128)(2,1)S(1)} copy-done((bf16[128,1024]{1,0:T(8,128)(2,1)S(1)}, bf16[128,1024]{1,0:T(8,128)(2,1)}, u32[]{:S(2)}) %copy-start.2) | copy-done | bytes 262168
  3.7 0.0 copy-start.3
  3.7 0.9 %copy-done.3 = bf16[1,128,512]{2,1,0:T(8,128)(2,1)S(1)} copy-done((bf16[1,128,512]{2,1,0:T(8,128)(2,1)S(1)}, bf16[1,128,512]{2,1,0:T(8,128)(2,1)}, u32[]{:S(2)}) %copy-start.3) | copy-done | bytes 131096
  4.6 0.0 copy-start.4
  4.6 0.9 %copy-done.4 = f32[2,32,512]{2,1,0:T(8,128)S(1)} copy-done((f32[2,32,512]{2,1,0:T(8,128)S(1)}, f32[2,32,512]{2,1,0:T(8,128)}, u32[]{:S(2)}) %copy-start.4) | copy-done | bytes 131096
  5.5 0.0 copy-start.5
  5.5 0.7 %copy-done.5 = bf16[1,128,64]{1,2,0:T(8,128)(2,1)S(1)} copy-done((bf16[1,128,64]{1,2,0:T(8,128)(2,1)S(1)}, bf16[1,128,64]{1,2,0:T(8,128)(2,1)}, u32[]{:S(2)}) %copy-start.5) | copy-done | bytes 16408
  6.2 0.0 copy-start.6
  6.2 0.7 %copy-done.6 = f32[512]{0:T(512)S(1)} copy-done((f32[512]{0:T(512)S(1)}, f32[512]{0:T(512)}, u32[]{:S(2)}) %copy-start.6) | copy-done | bytes 2072
  6.9 51.9 %shard_map.73 = bf16[128,2048]{1,0:T(8,128)(2,1)S(1)} custom-call(bf16[16,192,128]{2,1,0:T(8,128)(2,1)S(1)} %bitcast.10, bf16[128,512]{1,0:T(8,128)(2,1)S(1)} %bitcast.11, bf16[64,128]{1,0:T(8,128)(2,1)S(1)} %bitcast.12, f32[1,512]{1,0:T(1,128)S(1)} %bitcast.13, f32[2,32,512]{2,1,0:T(8,128)S(1)} %copy-done.4, bf16[128,1024]{1,0:T(8,128)(2,1)S(1)} %copy-done.2, ...), custom_call_target="tpu_custom_call" | custom-call | tf_op jit(solution)/shard_map/pallas_call | solution.py:370
  58.8 0.8 %copy.9 = bf16[1,128,2048]{2,1,0:T(8,128)(2,1)} copy(bf16[1,128,2048]{2,1,0:T(8,128)(2,1)S(1)} %bitcast.9) | data formatting | bytes 1048576
Async XLA Ops:
  0.0 1.6 %copy-start = (bf16[2048,512]{1,0:T(8,128)(2,1)S(1)}, bf16[2048,512]{1,0:T(8,128)(2,1)}, u32[]{:S(2)}) copy-start(bf16[2048,512]{1,0:T(8,128)(2,1)} %w_ref.1) | copy-start | bytes 6291460
  1.6 1.1 %copy-start.1 = (bf16[1,128,16,192]{1,3,2,0:T(8,128)(2,1)S(1)}, bf16[1,128,16,192]{1,3,2,0:T(8,128)(2,1)}, u32[]{:S(2)}) copy-start(bf16[1,128,16,192]{1,3,2,0:T(8,128)(2,1)} %param.7) | copy-start | bytes 2359300
  2.7 0.9 %copy-start.2 = (bf16[128,1024]{1,0:T(8,128)(2,1)S(1)}, bf16[128,1024]{1,0:T(8,128)(2,1)}, u32[]{:S(2)}) copy-start(bf16[128,1024]{1,0:T(8,128)(2,1)} %kvw_ref.1) | copy-start | bytes 786436
  3.7 0.9 %copy-start.3 = (bf16[1,128,512]{2,1,0:T(8,128)(2,1)S(1)}, bf16[1,128,512]{2,1,0:T(8,128)(2,1)}, u32[]{:S(2)}) copy-start(bf16[1,128,512]{2,1,0:T(8,128)(2,1)} %param.8) | copy-start | bytes 393220
  4.6 0.9 %copy-start.4 = (f32[2,32,512]{2,1,0:T(8,128)S(1)}, f32[2,32,512]{2,1,0:T(8,128)}, u32[]{:S(2)}) copy-start(f32[2,32,512]{2,1,0:T(8,128)} %constant.2.clone.table_ref) | copy-start | bytes 393220
  5.5 0.7 %copy-start.5 = (bf16[1,128,64]{1,2,0:T(8,128)(2,1)S(1)}, bf16[1,128,64]{1,2,0:T(8,128)(2,1)}, u32[]{:S(2)}) copy-start(bf16[1,128,64]{1,2,0:T(8,128)(2,1)} %param.9) | copy-start | bytes 49156
  6.2 0.7 %copy-start.6 = (f32[512]{0:T(512)S(1)}, f32[512]{0:T(512)}, u32[]{:S(2)}) copy-start(f32[512]{0:T(512)} %param.10) | copy-start | bytes 6148
where the time goes:
time: 59.9 us; the launch traced here: 59.6 us
  Pallas kernels  51.9 us (87%)
  local copies, waits for them, and re-layouts  7.67 us (13%)
    pallas_call x1, Pallas kernels, body(): pl.pallas_call(functools.partial(kernel, n, g, nx, hn, rope, width ** (-0...  51.9 us
    unnamed x15, local copies, waits for them, and re-layouts  7.67 us

commit v1 on v0

v1 whole, which is shorter than its diff:
```python
import functools
import math

import jax
import jax.numpy as jnp
import numpy as np
from jax import lax
from jax.experimental import pallas as pl
from jax.experimental.pallas import tpu as pltpu
from jax.sharding import PartitionSpec as P

NOPE = 128
VD = 128
LANES = 128
CORES = 2
UNITS = 16
LEAD = 3
LAG = 3
SPLIT = 2
VARIANTS = 4
MESH = pl.DeviceIdType.MESH


def rotation_table(length, rope):
    half = rope // 2
    inverse = np.power(10000.0, -np.arange(half) * 2.0 / rope).astype(np.float32)
    angle = inverse[:, None] * np.arange(length, dtype=np.float32)[None, :]
    return np.stack([np.cos(angle), np.sin(angle)]).astype(np.float32)


def kernel(
    n, g, nx, p, hn, rope, scale, sub,
    q_ref, latent_ref, key_ref, gain_ref, table_ref, kvw_ref, w_ref, out_ref,
    qbuf, lat, rkey, shared, kvw, wfull, attout, attin, acc, latin, keyin, gain, table,
    loc, l_s, l_r, r_s, r_r, q_s, q_r, kz_s, kz_r, a_s, a_r,
    kx_s, kx_r, ky_s, ky_r, kc_s, kc_r, ko_s, ko_r,
    wx_s, wx_r, wy_s, wy_r, wc_s, wc_r, wo_s, wo_r,
):
    me = lax.axis_index("sp")
    y = lax.axis_index("grp")
    dp = lax.axis_index("dp")
    x, c = dp // CORES, dp % CORES
    b, r = lax.div(me, p), lax.rem(me, p)
    m = n // p
    ndp = nx * CORES
    tok, latw = latent_ref.shape
    half = rope // 2
    rrows = rkey.shape[1]
    krows = kvw_ref.shape[0]
    kh = krows // g
    cols = w_ref.shape[1]
    kd = hn * VD
    part = kd // g
    crow = part // sub
    units = n * sub
    length = n * tok
    wide = NOPE + VD

    def chip(xx, cc):
        return {"dp": xx * CORES + cc}

    partner = chip(x, 1 - c)

    def remote(src, dst, ss, rs, dev):
        return pltpu.make_async_remote_copy(
            src_ref=src, dst_ref=dst, send_sem=ss, recv_sem=rs, device_id=dev, device_id_type=MESH
        )

    def span(start, size):
        return pl.ds(pl.multiple_of(start, size), size)

    def mate(s):
        return lax.rem(r + s, p)

    def group(o):
        return lax.rem(b + o, m)

    def xs(o):
        return lax.rem(x + nx - o, nx) * CORES + c

    get_lat = pltpu.make_async_copy(latent_ref, latin, loc.at[0])
    get_key = pltpu.make_async_copy(key_ref, keyin, loc.at[1])
    get_gain = pltpu.make_async_copy(gain_ref, gain, loc.at[2])
    get_table = pltpu.make_async_copy(table_ref.at[:, :, span(b * (p * tok), p * tok)], table, loc.at[3])
    own_k = pltpu.make_async_copy(kvw_ref, kvw.at[b, span(dp * krows, krows)], loc.at[4])
    own_w = pltpu.make_async_copy(w_ref, wfull.at[dp], loc.at[5])

    def own_q(i):
        return pltpu.make_async_copy(q_ref.at[span((r + p * i) * hn, hn)], qbuf.at[r, i], loc.at[6 + i])

    for copy in (get_lat, get_key, get_gain, get_table):
        copy.start()

    barrier = pltpu.get_barrier_semaphore()
    for o in range(1, n):
        pl.semaphore_signal(barrier, 1, device_id={"sp": lax.rem(me + o, n)}, device_id_type=MESH)
    for o in range(1, nx):
        pl.semaphore_signal(barrier, 1, device_id=chip(lax.rem(x + o, nx), c), device_id_type=MESH)
    for o in range(1, g):
        pl.semaphore_signal(barrier, 1, device_id={"grp": lax.rem(y + o, g)}, device_id_type=MESH)
    pl.semaphore_signal(barrier, 1, device_id=partner, device_id_type=MESH)

    own_k.start()
    for i in range(m):
        own_q(i).start()
    own_w.start()

    def turned(values, cosine, sine):
        first, second = values[:half].astype(jnp.float32), values[half:].astype(jnp.float32)
        return first * cosine - second * sine, first * sine + second * cosine

    get_lat.wait()
    get_gain.wait()
    latent = latin[...].astype(jnp.float32)
    square = jnp.mean(latent * latent, axis=-1, keepdims=True)
    lat[span(me * tok, tok), :] = (latent * lax.rsqrt(square + 1e-06) * gain[...]).astype(jnp.bfloat16)
    get_key.wait()
    get_table.wait()
    mine = span(r * tok, tok)
    first, second = turned(keyin[...], table[0, :, mine], table[1, :, mine])
    both = jnp.concatenate([first, second], axis=0).astype(jnp.bfloat16)
    for f in range(rope // rrows):
        rkey[me, :, f * tok : (f + 1) * tok] = both[f * rrows : (f + 1) * rrows]

    pl.semaphore_wait(barrier, (n - 1) + (nx - 1) + (g - 1) + 1)

    def kz_copy(o):
        return remote(
            kvw_ref, kvw.at[b, span(dp * krows, krows)], kz_s.at[o - 1], kz_r.at[o - 1],
            {"sp": group(o) * p + r},
        )

    def lat_copies(o):
        to = {"sp": lax.rem(me + o, n)}
        rows = span(me * tok, tok)
        return (
            remote(lat.at[rows], lat.at[rows], l_s.at[o - 1], l_r.at[o - 1], to),
            remote(rkey.at[me], rkey.at[me], r_s.at[o - 1], r_r.at[o - 1], to),
        )

    def lat_sent(o):
        return lax.rem(me + o, n) >= b * p

    def lat_taken(o):
        return lax.rem(me + n - o, n) < (b + 1) * p

    def q_copy(s, e):
        t, i = mate(s), group(e)
        return remote(
            q_ref.at[span((t + p * i) * hn, hn)], qbuf.at[r, i], q_s.at[s - 1, i], q_r.at[s - 1, i],
            {"sp": b * p + t},
        )

    def a_copy(s, i, h):
        t = mate(s)
        return remote(
            attout.at[i, t, h], attin.at[r, i, h], a_s.at[s - 1, i, h], a_r.at[s - 1, i, h],
            {"sp": b * p + t},
        )

    def k_rows(i, d, q):
        return kvw.at[i, span(d * krows + q * kh, kh)]

    def k_x(o, e):
        i = group(e)
        src = kvw_ref.at[span(y * kh, kh)] if e == 0 else k_rows(i, dp, y)
        return remote(
            src, k_rows(i, dp, y), kx_s.at[o - 1, e], kx_r.at[o - 1, e], chip(lax.rem(x + o, nx), c)
        )

    def k_y(o, q, e):
        ref = k_rows(group(e), xs(o), y)
        return remote(
            ref, ref, ky_s.at[o - 1, q - 1, e], ky_r.at[o - 1, q - 1, e], {"grp": lax.rem(y + q, g)}
        )

    def k_c(o, q, e):
        ref = k_rows(group(e), xs(o), lax.rem(y + g - q, g))
        return remote(ref, ref, kc_s.at[o - 1, q, e], kc_r.at[o - 1, q, e], partner)

    def k_own(e):
        dst = kvw.at[group(e), span(dp * krows, krows)]
        return remote(kvw_ref if e == 0 else dst, dst, ko_s.at[e], ko_r.at[e], partner)

    def place(k):
        return lax.rem(r + k % p, p), group(k // p)

    def w_rows(yy, u):
        q, i = place(u // sub)
        return span((q + p * i) * kd + yy * part + (u % sub) * crow, crow)

    def w_x(o, u):
        rows = w_rows(y, u)
        return remote(
            w_ref.at[rows], wfull.at[dp, rows], wx_s.at[o - 1, u], wx_r.at[o - 1, u],
            chip(lax.rem(x + o, nx), c),
        )

    def w_y(o, q, u):
        ref = wfull.at[xs(o), w_rows(y, u)]
        return remote(
            ref, ref, wy_s.at[o - 1, q - 1, u], wy_r.at[o - 1, q - 1, u], {"grp": lax.rem(y + q, g)}
        )

    def w_c(o, q, u):
        ref = wfull.at[xs(o), w_rows(lax.rem(y + g - q, g), u)]
        return remote(ref, ref, wc_s.at[o - 1, q, u], wc_r.at[o - 1, q, u], partner)

    w_own = remote(w_ref, wfull.at[dp], wo_s, wo_r, partner)

    items = []
    for u in range(units):
        if u * m % units < m:
            items.append(("k", u * m // units))
        items.append(("w", u))

    def issue(s):
        if s >= len(items):
            return
        kind, e = items[s]
        if kind == "k":
            if e > 0:
                kz_copy(m - e).wait_recv()
            for o in range(1, nx):
                k_x(o, e).start()
            k_own(e).start()
        else:
            for o in range(1, nx):
                w_x(o, e).start()

    def pass_x(s):
        if s >= len(items):
            return
        kind, e = items[s]
        in_x, in_y, in_c = (k_x, k_y, k_c) if kind == "k" else (w_x, w_y, w_c)
        for o in range(1, nx):
            in_x(o, e).wait_recv()
            for q in range(1, g):
                in_y(o, q, e).start()
            in_c(o, 0, e).start()

    def pass_y(s):
        if s < 0 or s >= len(items):
            return
        kind, e = items[s]
        in_y, in_c = (k_y, k_c) if kind == "k" else (w_y, w_c)
        for o in range(1, nx):
            for q in range(1, g):
                in_y(o, q, e).wait_recv()
                in_c(o, q, e).start()

    done = []

    def step():
        s = len(done)
        done.append(s)
        issue(s + LEAD)
        pass_x(s)
        pass_y(s - LAG)

    for o in range(1, m):
        kz_copy(o).start()
    issue(0)
    for o in range(1, n):
        @pl.when(lat_sent(o))
        def _():
            for copy in lat_copies(o):
                copy.start()
    for e in range(m):
        for s in range(1, p):
            q_copy(s, e).start()
    for s in range(1, LEAD):
        issue(s)
    w_own.start()

    before = len(items) // 2 + 1
    for s in range(before):
        step()

    for o in range(1, n):
        @pl.when(lat_taken(o))
        def _():
            for copy in lat_copies(o):
                copy.wait_recv()

    @pl.loop(0, (b + 1) * p)
    def _(j):
        turn = jnp.concatenate(
            [rkey[j, :, f * tok : (f + 1) * tok] for f in range(rope // rrows)], axis=0
        ).astype(jnp.float32)
        filled = jnp.concatenate([turn, jnp.zeros((LANES - rope, tok), jnp.float32)], axis=0)
        shared[span(j * tok, tok), :] = filled.T.astype(jnp.bfloat16)

    variants = math.gcd(VARIANTS, m)
    stride = length // variants
    if stride > p * tok:
        @pl.loop((b + 1) * p, n)
        def _(j):
            rows = span(j * tok, tok)
            lat[rows, :] = jnp.zeros((tok, latw), lat.dtype)
            shared[rows, :] = jnp.zeros((tok, LANES), shared.dtype)

    def head_over(i, h, extent):
        row = lax.broadcasted_iota(jnp.int32, (stride, p * tok), 0)
        col = lax.broadcasted_iota(jnp.int32, (stride, p * tok), 1)
        kept = row - col <= b * (p * tok) - (extent - stride)
        both = jnp.dot(
            lat[:extent, :], kvw[i, :, h * wide : (h + 1) * wide], preferred_element_type=jnp.float32
        )
        keys = jnp.concatenate([both[:, :NOPE].astype(jnp.bfloat16), shared[:extent, :]], axis=1)
        values = both[:, NOPE:].T.astype(jnp.bfloat16)
        raw = jnp.concatenate([qbuf[t, i, h, :, :] for t in range(p)], axis=1)
        first, second = turned(raw[NOPE:], table[0], table[1])
        query = jnp.concatenate(
            [
                raw[:NOPE], first.astype(jnp.bfloat16), second.astype(jnp.bfloat16),
                jnp.zeros((LANES - rope, p * tok), jnp.bfloat16),
            ],
            axis=0,
        )
        s = jnp.dot(keys, query, preferred_element_type=jnp.float32)
        last = jnp.where(kept, s[extent - stride :], -jnp.inf)
        s = last if extent == stride else jnp.concatenate([s[: extent - stride], last], axis=0)
        top = jnp.max(s, axis=0, keepdims=True)
        e = jnp.exp2((s - top) * (scale * math.log2(math.e)))
        probs = (e * (1.0 / jnp.sum(e, axis=0, keepdims=True))).astype(jnp.bfloat16)
        o = jnp.dot(values, probs, preferred_element_type=jnp.float32)
        for t in range(p):
            attout[i, t, h] = o[:, t * tok : (t + 1) * tok].T.astype(jnp.bfloat16)

    def head(i, h):
        for v in range(variants):
            @pl.when(lax.div(b, m // variants) == v)
            def _():
                head_over(i, h, (v + 1) * stride)

    def take_q(e):
        i = group(e)
        own_q(i).wait()
        for s in range(1, p):
            q_copy(s, e).wait_recv()

    def take_k(e):
        k_own(e).wait_recv()
        for o in range(1, nx):
            for q in range(g):
                k_c(o, q, e).wait_recv()

    own_k.wait()
    if m * hn <= 2 * VARIANTS:
        for e in range(m):
            if e > 0:
                while len(done) <= items.index(("k", e)) + LAG:
                    step()
            take_q(e)
            take_k(e)
            for h in range(hn):
                head(group(e), h)
                for s in range(1, p):
                    a_copy(s, group(e), h).start()
                step()
        while len(done) < len(items) + LAG:
            step()
    else:
        while len(done) < len(items) + LAG:
            step()
        for e in range(m):
            take_q(e)
            take_k(e)

        @pl.loop(0, m)
        def _(e):
            i = lax.rem(b + e, m)
            for h in range(hn):
                head(i, h)
                for s in range(1, p):
                    a_copy(s, i, h).start()

    own_w.wait()
    w_own.wait_recv()

    for k in range(n):
        for u in range(k * sub, (k + 1) * sub):
            for o in range(1, nx):
                for q in range(g):
                    w_c(o, q, u).wait_recv()
        q, i = place(k)
        if k % p == 0:
            block = jnp.concatenate([attout[i, r, h] for h in range(hn)], axis=1)
        else:
            for h in range(hn):
                a_copy(p - k % p, i, h).wait_recv()
            block = jnp.concatenate([attin[q, i, h] for h in range(hn)], axis=1)
        rows = span((q + p * i) * kd, kd)
        for d in range(ndp):
            part_sum = jnp.dot(block, wfull[d, rows, :], preferred_element_type=jnp.float32)
            where = slice(d * cols, (d + 1) * cols)
            if k == 0:
                acc[:, where] = part_sum
            elif k < n - 1:
                acc[:, where] += part_sum
            else:
                out_ref[:, where] = (acc[:, where] + part_sum).astype(out_ref.dtype)

    for o in range(1, n):
        @pl.when(lat_sent(o))
        def _():
            for copy in lat_copies(o):
                copy.wait_send()
    for o in range(1, m):
        kz_copy(o).wait_send()
    for e in range(m):
        k_own(e).wait_send()
        for s in range(1, p):
            q_copy(s, e).wait_send()
            for h in range(hn):
                a_copy(s, group(e), h).wait_send()
    w_own.wait_send()
    for kind, e in items:
        in_x, in_y, in_c = (k_x, k_y, k_c) if kind == "k" else (w_x, w_y, w_c)
        for o in range(1, nx):
            in_x(o, e).wait_send()
            for q in range(1, g):
                in_y(o, q, e).wait_send()
            for q in range(g):
                in_c(o, q, e).wait_send()


def body(sizes, queries, kv_latent, rope_key, kv_gain, kv_weight, out_weight):
    g, n, dp = sizes
    nx = dp // CORES
    tok, heads, width = queries.shape[1:]
    rope = width - NOPE
    hn = heads // n
    latw = kv_latent.shape[2]
    p = math.gcd(SPLIT, n)
    m = n // p
    sub = max(1, UNITS // n)
    units = n * sub
    q = jnp.transpose(queries[0], (1, 2, 0))
    key = jnp.transpose(rope_key[0])
    table = jnp.asarray(rotation_table(n * tok, rope))

    d_in, cols = out_weight.shape
    kcols = kv_weight.shape[1]
    dma = pltpu.SemaphoreType.DMA
    bf = jnp.bfloat16
    xn = max(nx - 1, 1)
    gn = max(g - 1, 1)
    pn = max(p - 1, 1)
    mn = max(m - 1, 1)
    vmem = pl.BlockSpec(memory_space=pltpu.VMEM)
    hbm = pl.BlockSpec(memory_space=pltpu.HBM)
    out = pl.pallas_call(
        functools.partial(kernel, n, g, nx, p, hn, rope, width**-0.5, sub),
        out_shape=jax.ShapeDtypeStruct((tok, cols * dp), bf),
        in_specs=[hbm] * 7,
        out_specs=vmem,
        scratch_shapes=[
            pltpu.VMEM((p, m, hn, width, tok), bf),
            pltpu.VMEM((n * tok, latw), bf),
            pltpu.VMEM((n, rope * tok // latw, latw), bf),
            pltpu.VMEM((n * tok, LANES), bf),
            pltpu.VMEM((m, kv_weight.shape[0] * dp, kcols), bf),
            pltpu.VMEM((dp, d_in, cols), bf),
            pltpu.VMEM((m, p, hn, tok, VD), bf),
            pltpu.VMEM((p, m, hn, tok, VD), bf),
            pltpu.VMEM((tok, cols * dp), jnp.float32),
            pltpu.VMEM((tok, latw), bf),
            pltpu.VMEM((rope, tok), bf),
            pltpu.VMEM((1, latw), jnp.float32),
            pltpu.VMEM((2, rope // 2, p * tok), jnp.float32),
            dma((6 + m,)),
            dma((n,)), dma((n,)), dma((n,)), dma((n,)),
            dma((pn, m)), dma((pn, m)),
            dma((mn,)), dma((mn,)),
            dma((pn, m, hn)), dma((pn, m, hn)),
            dma((xn, m)), dma((xn, m)),
            dma((xn, gn, m)), dma((xn, gn, m)),
            dma((xn, g, m)), dma((xn, g, m)),
            dma((m,)), dma((m,)),
            dma((xn, units)), dma((xn, units)),
            dma((xn, gn, units)), dma((xn, gn, units)),
            dma((xn, g, units)), dma((xn, g, units)),
            dma(()), dma(()),
        ],
        compiler_params=pltpu.CompilerParams(
            collective_id=0, has_side_effects=True, vmem_limit_bytes=60 * 1024 * 1024
        ),
    )(q, kv_latent[0], key, kv_gain[None], table, kv_weight, out_weight)
    return out[None]


def solution(mesh):
    sizes = (mesh.shape["grp"], mesh.shape["sp"], mesh.shape["dp"])
    return jax.shard_map(
        functools.partial(body, sizes),
        mesh=mesh,
        in_specs=(
            P(("grp", "dp"), "sp", None, None),
            P(("grp", "dp"), "sp", None),
            P(("grp", "dp"), "sp", None),
            P(),
            P("dp", "sp"),
            P(None, "dp"),
        ),
        out_specs=P(("grp", "dp"), "sp", None),
        check_vma=False,
    )
```

time: 59.9 us -> 49.4 us (0.82)
  the two profiles are of different devices: /device:TPU:0 before, /device:TPU:25 now
where the time goes in v1:
time: 49.4 us; the launch traced here: 49.2 us
  Pallas kernels  47.3 us (96%)
  local copies, waits for them, and re-layouts  1.88 us (4%)
    pallas_call x1, Pallas kernels, body(): pl.pallas_call(functools.partial(kernel, n, g, nx, p, hn, rope, width **...  47.3 us
    unnamed x1, local copies, waits for them, and re-layouts  1.88 us

profile of v1, /device:TPU:25, one launch (start us, length us, event | category | flops | bytes accessed | tf_op | source)
XLA Modules:
  0.0 49.2 jit_solution(12633637953288472873)
XLA Ops:
  0.0 47.3 %shard_map.73 = bf16[128,2048]{1,0:T(8,128)(2,1)} custom-call(bf16[16,192,128]{2,1,0:T(8,128)(2,1)} %bitcast.10, bf16[128,512]{1,0:T(8,128)(2,1)} %bitcast.11, bf16[64,128]{1,0:T(8,128)(2,1)} %bitcast.12, f32[1,512]{1,0:T(1,128)} %bitcast.13, f32[2,32,512]{2,1,0:T(8,128)} %constant.2.clone.table_ref, bf16[128,1024]{1,0:T(8,128)(2,1)} %kvw_ref.1, ...), custom_call_target="tpu_custom_call" | custom-call | tf_op jit(solution)/shard_map/pallas_call | solution.py:454
  47.3 1.9 %copy.9 = bf16[1,128,2048]{2,1,0:T(8,128)(2,1)} copy(bf16[1,128,2048]{2,1,0:T(8,128)(2,1)} %bitcast.9) | data formatting | bytes 1048576

commit v2 on v1

--- a/solution.py
+++ b/solution.py
@@ -14,8 +14,14 @@
 LANES = 128
 CORES = 2
 UNITS = 16
-LEAD = 3
-LAG = 3
+LEAD = 4
+LAG = 4
+KEYS = 7
+RELAY = 8
+LATE = 12
+START = 12
+DIRECT = 1
+PLAN = (1, 1, 1, 1, 2, 2, 1, 1, 1)
 SPLIT = 2
 VARIANTS = 4
 MESH = pl.DeviceIdType.MESH
@@ -32,9 +38,9 @@
     n, g, nx, p, hn, rope, scale, sub,
     q_ref, latent_ref, key_ref, gain_ref, table_ref, kvw_ref, w_ref, out_ref,
     qbuf, lat, rkey, shared, kvw, wfull, attout, attin, acc, latin, keyin, gain, table,
-    loc, l_s, l_r, r_s, r_r, q_s, q_r, kz_s, kz_r, a_s, a_r,
+    loc, lm_s, lm_r, lg_s, lg_r, lr_s, lr_r, q_s, q_r, kz_s, kz_r, a_s, a_r,
     kx_s, kx_r, ky_s, ky_r, kc_s, kc_r, ko_s, ko_r,
-    wx_s, wx_r, wy_s, wy_r, wc_s, wc_r, wo_s, wo_r,
+    wx_s, wx_r, wy_s, wy_r, wc_s, wc_r, wo_s, wo_r, far,
 ):
     me = lax.axis_index("sp")
     y = lax.axis_index("grp")
@@ -92,8 +98,25 @@
         copy.start()
 
     barrier = pltpu.get_barrier_semaphore()
-    for o in range(1, n):
-        pl.semaphore_signal(barrier, 1, device_id={"sp": lax.rem(me + o, n)}, device_id_type=MESH)
+    staged = (m - 1) * p == 2
+
+    def greet(semaphore):
+        @pl.when(me > 0)
+        def _():
+            pl.semaphore_signal(semaphore, 1, device_id={"sp": me - 1}, device_id_type=MESH)
+
+        @pl.when(me < n - 1)
+        def _():
+            pl.semaphore_signal(semaphore, 1, device_id={"sp": me + 1}, device_id_type=MESH)
+
+    beside = jnp.where(me > 0, 1, 0) + jnp.where(me < n - 1, 1, 0)
+    if staged:
+        greet(barrier)
+    else:
+        for s in range(1, p):
+            pl.semaphore_signal(barrier, 1, device_id={"sp": b * p + mate(s)}, device_id_type=MESH)
+        for o in range(1, m):
+            pl.semaphore_signal(barrier, 1, device_id={"sp": group(o) * p + r}, device_id_type=MESH)
     for o in range(1, nx):
         pl.semaphore_signal(barrier, 1, device_id=chip(lax.rem(x + o, nx), c), device_id_type=MESH)
     for o in range(1, g):
@@ -108,6 +131,187 @@
     def turned(values, cosine, sine):
         first, second = values[:half].astype(jnp.float32), values[half:].astype(jnp.float32)
         return first * cosine - second * sine, first * sine + second * cosine
+
+    def kz_copy(o, q):
+        part_of = lax.rem(y + q, g)
+        return remote(
+            kvw_ref.at[span(part_of * kh, kh)], k_rows(b, dp, part_of),
+            kz_s.at[o - 1, q], kz_r.at[o - 1, q], {"sp": group(o) * p + r},
+        )
+
+    def lat_pair(j, to, ss, rs):
+        rows = span(j * tok, tok)
+        return (
+            remote(lat.at[rows], lat.at[rows], ss.at[0], rs.at[0], {"sp": to}),
+            remote(rkey.at[j], rkey.at[j], ss.at[1], rs.at[1], {"sp": to}),
+        )
+
+    def lat_mate(s):
+        return lat_pair(me, b * p + mate(s), lm_s.at[s - 1], lm_r.at[s - 1])
+
+    def lat_group(o):
+        return lat_pair(me, group(o) * p + r, lg_s.at[o - 1], lg_r.at[o - 1])
+
+    def lat_relay(o, s):
+        j = lax.rem(b + m - o, m) * p + r
+        return lat_pair(j, b * p + mate(s), lr_s.at[o - 1, s - 1], lr_r.at[o - 1, s - 1])
+
+    def relay():
+        for o in range(1, m):
+            @pl.when(b - o >= 0)
+            def _():
+                for copy in lat_group(o):
+                    copy.wait_recv()
+                for s in range(1, p):
+                    for copy in lat_relay(o, s):
+                        copy.start()
+
+    def q_copy(s, e):
+        t, i = mate(s), group(e)
+        return remote(
+            q_ref.at[span((t + p * i) * hn, hn)], qbuf.at[r, i], q_s.at[s - 1, i], q_r.at[s - 1, i],
+            {"sp": b * p + t},
+        )
+
+    def a_copy(s, i, h):
+        t = mate(s)
+        return remote(
+            attout.at[i, t, h], attin.at[r, i, h], a_s.at[s - 1, i, h], a_r.at[s - 1, i, h],
+            {"sp": b * p + t},
+        )
+
+    def k_rows(i, d, q):
+        return kvw.at[i, span(d * krows + q * kh, kh)]
+
+    def k_x(o, e):
+        dst = k_rows(group(e), dp, y)
+        src = kvw_ref.at[span(y * kh, kh)] if e == 0 else dst
+        return remote(
+            src, dst, kx_s.at[o - 1, e], kx_r.at[o - 1, e], chip(lax.rem(x + o, nx), c)
+        )
+
+    def k_y(o, q, e):
+        ref = k_rows(group(e), xs(o), y)
+        return remote(
+            ref, ref, ky_s.at[o - 1, q - 1, e], ky_r.at[o - 1, q - 1, e], {"grp": lax.rem(y + q, g)}
+        )
+
+    def k_c(o, q, e):
+        ref = k_rows(group(e), xs(o), lax.rem(y + g - q, g))
+        return remote(ref, ref, kc_s.at[o - 1, q, e], kc_r.at[o - 1, q, e], partner)
+
+    def k_own(q, e):
+        part_of = lax.rem(y + q, g)
+        dst = k_rows(group(e), dp, part_of)
+        src = kvw_ref.at[span(part_of * kh, kh)] if e == 0 else dst
+        return remote(src, dst, ko_s.at[q, e], ko_r.at[q, e], partner)
+
+    def late():
+        for e in range(1, m):
+            for q in range(1, g):
+                kz_copy(m - e, q).wait_recv()
+                k_own(q, e).start()
+
+    def place(k):
+        return lax.rem(r + k % p, p), group(k // p)
+
+    def w_rows(yy, u):
+        q, i = place(u // sub)
+        return span((q + p * i) * kd + yy * part + (u % sub) * crow, crow)
+
+    def direct(kind, u):
+        return kind == "w" and u >= units - DIRECT
+
+    def w_x(o, u, q=0):
+        rows = w_rows(lax.rem(y + g - q, g), u)
+        sems = (wx_s.at[o - 1, u], wx_r.at[o - 1, u])
+        if q > 0:
+            sems = (wy_s.at[o - 1, q - 1, u], wy_r.at[o - 1, q - 1, u])
+        return remote(w_ref.at[rows], wfull.at[dp, rows], *sems, chip(lax.rem(x + o, nx), c))
+
+    def w_y(o, q, u):
+        ref = wfull.at[xs(o), w_rows(y, u)]
+        return remote(
+            ref, ref, wy_s.at[o - 1, q - 1, u], wy_r.at[o - 1, q - 1, u], {"grp": lax.rem(y + q, g)}
+        )
+
+    def w_c(o, q, u):
+        ref = wfull.at[xs(o), w_rows(lax.rem(y + g - q, g), u)]
+        return remote(ref, ref, wc_s.at[o - 1, q, u], wc_r.at[o - 1, q, u], partner)
+
+    w_own = remote(w_ref, wfull.at[dp], wo_s, wo_r, partner)
+
+    items = [("w", u) for u in range(units)]
+    for e in range(1, m):
+        items.insert(KEYS + (e - 1) * (units - KEYS) // (m - 1), ("k", e))
+    items.insert(1, ("k", 0))
+
+    def issue(s):
+        if s >= len(items):
+            return
+        kind, e = items[s]
+        if kind == "k":
+            if e > 0:
+                kz_copy(m - e, 0).wait_recv()
+            for o in range(1, nx):
+                k_x(o, e).start()
+            for q in range(g if e == 0 else 1):
+                k_own(q, e).start()
+        else:
+            for o in range(1, nx):
+                for q in range(g if direct(kind, e) else 1):
+                    w_x(o, e, q).start()
+
+    def pass_x(s):
+        if s >= len(items):
+            return
+        kind, e = items[s]
+        for o in range(1, nx):
+            if direct(kind, e):
+                for q in range(g):
+                    w_x(o, e, q).wait_recv()
+                    w_c(o, q, e).start()
+                continue
+            in_x, in_y, in_c = (k_x, k_y, k_c) if kind == "k" else (w_x, w_y, w_c)
+            in_x(o, e).wait_recv()
+            for q in range(1, g):
+                in_y(o, q, e).start()
+            in_c(o, 0, e).start()
+
+    def pass_y(s):
+        if s < 0 or s >= len(items) or direct(*items[s]):
+            return
+        kind, e = items[s]
+        in_y, in_c = (k_y, k_c) if kind == "k" else (w_y, w_c)
+        for o in range(1, nx):
+            for q in range(1, g):
+                in_y(o, q, e).wait_recv()
+                in_c(o, q, e).start()
+
+    done = []
+
+    def step():
+        s = len(done)
+        if s >= len(items) + LAG:
+            return
+        done.append(s)
+        if s == RELAY:
+            relay()
+            for e in range(1, m):
+                for o in range(1, p):
+                    q_copy(o, e).start()
+        if s == LATE:
+            late()
+        issue(s + LEAD)
+        pass_x(s)
+        pass_y(s - LAG)
+
+    along = beside if staged else (p - 1) + (m - 1)
+    pl.semaphore_wait(barrier, along + (nx - 1) + (g - 1) + 1)
+    if staged:
+        greet(far)
+    for s in range(LEAD):
+        issue(s)
 
     get_lat.wait()
     get_gain.wait()
@@ -122,166 +326,37 @@
     for f in range(rope // rrows):
         rkey[me, :, f * tok : (f + 1) * tok] = both[f * rrows : (f + 1) * rrows]
 
-    pl.semaphore_wait(barrier, (n - 1) + (nx - 1) + (g - 1) + 1)
-
-    def kz_copy(o):
-        return remote(
-            kvw_ref, kvw.at[b, span(dp * krows, krows)], kz_s.at[o - 1], kz_r.at[o - 1],
-            {"sp": group(o) * p + r},
-        )
-
-    def lat_copies(o):
-        to = {"sp": lax.rem(me + o, n)}
-        rows = span(me * tok, tok)
-        return (
-            remote(lat.at[rows], lat.at[rows], l_s.at[o - 1], l_r.at[o - 1], to),
-            remote(rkey.at[me], rkey.at[me], r_s.at[o - 1], r_r.at[o - 1], to),
-        )
-
-    def lat_sent(o):
-        return lax.rem(me + o, n) >= b * p
-
-    def lat_taken(o):
-        return lax.rem(me + n - o, n) < (b + 1) * p
-
-    def q_copy(s, e):
-        t, i = mate(s), group(e)
-        return remote(
-            q_ref.at[span((t + p * i) * hn, hn)], qbuf.at[r, i], q_s.at[s - 1, i], q_r.at[s - 1, i],
-            {"sp": b * p + t},
-        )
-
-    def a_copy(s, i, h):
-        t = mate(s)
-        return remote(
-            attout.at[i, t, h], attin.at[r, i, h], a_s.at[s - 1, i, h], a_r.at[s - 1, i, h],
-            {"sp": b * p + t},
-        )
-
-    def k_rows(i, d, q):
-        return kvw.at[i, span(d * krows + q * kh, kh)]
-
-    def k_x(o, e):
-        i = group(e)
-        src = kvw_ref.at[span(y * kh, kh)] if e == 0 else k_rows(i, dp, y)
-        return remote(
-            src, k_rows(i, dp, y), kx_s.at[o - 1, e], kx_r.at[o - 1, e], chip(lax.rem(x + o, nx), c)
-        )
-
-    def k_y(o, q, e):
-        ref = k_rows(group(e), xs(o), y)
-        return remote(
-            ref, ref, ky_s.at[o - 1, q - 1, e], ky_r.at[o - 1, q - 1, e], {"grp": lax.rem(y + q, g)}
-        )
-
-    def k_c(o, q, e):
-        ref = k_rows(group(e), xs(o), lax.rem(y + g - q, g))
-        return remote(ref, ref, kc_s.at[o - 1, q, e], kc_r.at[o - 1, q, e], partner)
-
-    def k_own(e):
-        dst = kvw.at[group(e), span(dp * krows, krows)]
-        return remote(kvw_ref if e == 0 else dst, dst, ko_s.at[e], ko_r.at[e], partner)
-
-    def place(k):
-        return lax.rem(r + k % p, p), group(k // p)
-
-    def w_rows(yy, u):
-        q, i = place(u // sub)
-        return span((q + p * i) * kd + yy * part + (u % sub) * crow, crow)
-
-    def w_x(o, u):
-        rows = w_rows(y, u)
-        return remote(
-            w_ref.at[rows], wfull.at[dp, rows], wx_s.at[o - 1, u], wx_r.at[o - 1, u],
-            chip(lax.rem(x + o, nx), c),
-        )
-
-    def w_y(o, q, u):
-        ref = wfull.at[xs(o), w_rows(y, u)]
-        return remote(
-            ref, ref, wy_s.at[o - 1, q - 1, u], wy_r.at[o - 1, q - 1, u], {"grp": lax.rem(y + q, g)}
-        )
-
-    def w_c(o, q, u):
-        ref = wfull.at[xs(o), w_rows(lax.rem(y + g - q, g), u)]
-        return remote(ref, ref, wc_s.at[o - 1, q, u], wc_r.at[o - 1, q, u], partner)
-
-    w_own = remote(w_ref, wfull.at[dp], wo_s, wo_r, partner)
-
-    items = []
-    for u in range(units):
-        if u * m % units < m:
-            items.append(("k", u * m // units))
-        items.append(("w", u))
-
-    def issue(s):
-        if s >= len(items):
-            return
-        kind, e = items[s]
-        if kind == "k":
-            if e > 0:
-                kz_copy(m - e).wait_recv()
-            for o in range(1, nx):
-                k_x(o, e).start()
-            k_own(e).start()
-        else:
-            for o in range(1, nx):
-                w_x(o, e).start()
-
-    def pass_x(s):
-        if s >= len(items):
-            return
-        kind, e = items[s]
-        in_x, in_y, in_c = (k_x, k_y, k_c) if kind == "k" else (w_x, w_y, w_c)
-        for o in range(1, nx):
-            in_x(o, e).wait_recv()
-            for q in range(1, g):
-                in_y(o, q, e).start()
-            in_c(o, 0, e).start()
-
-    def pass_y(s):
-        if s < 0 or s >= len(items):
-            return
-        kind, e = items[s]
-        in_y, in_c = (k_y, k_c) if kind == "k" else (w_y, w_c)
-        for o in range(1, nx):
-            for q in range(1, g):
-                in_y(o, q, e).wait_recv()
-                in_c(o, q, e).start()
-
-    done = []
-
-    def step():
-        s = len(done)
-        done.append(s)
-        issue(s + LEAD)
-        pass_x(s)
-        pass_y(s - LAG)
-
+    if staged:
+        pl.semaphore_wait(far, beside)
     for o in range(1, m):
-        kz_copy(o).start()
-    issue(0)
-    for o in range(1, n):
-        @pl.when(lat_sent(o))
+        kz_copy(o, 0).start()
+    for o in range(1, m):
+        @pl.when(b + o < m)
         def _():
-            for copy in lat_copies(o):
+            for copy in lat_group(o):
                 copy.start()
-    for e in range(m):
-        for s in range(1, p):
-            q_copy(s, e).start()
-    for s in range(1, LEAD):
-        issue(s)
+    for s in range(1, p):
+        for copy in lat_mate(s):
+            copy.start()
+    for o in range(1, m):
+        for q in range(1, g):
+            kz_copy(o, q).start()
+    for s in range(1, p):
+        q_copy(s, 0).start()
     w_own.start()
 
-    before = len(items) // 2 + 1
-    for s in range(before):
+    for s in range(START):
         step()
 
-    for o in range(1, n):
-        @pl.when(lat_taken(o))
+    for s in range(1, p):
+        for copy in lat_mate(s):
+            copy.wait_recv()
+    for o in range(1, m):
+        @pl.when(b - o >= 0)
         def _():
-            for copy in lat_copies(o):
-                copy.wait_recv()
+            for s in range(1, p):
+                for copy in lat_relay(o, s):
+                    copy.wait_recv()
 
     @pl.loop(0, (b + 1) * p)
     def _(j):
@@ -341,45 +416,28 @@
             q_copy(s, e).wait_recv()
 
     def take_k(e):
-        k_own(e).wait_recv()
+        for q in range(g):
+            k_own(q, e).wait_recv()
         for o in range(1, nx):
             for q in range(g):
                 k_c(o, q, e).wait_recv()
 
-    own_k.wait()
-    if m * hn <= 2 * VARIANTS:
-        for e in range(m):
-            if e > 0:
-                while len(done) <= items.index(("k", e)) + LAG:
-                    step()
+    def attend(e, h):
+        if h == 0:
+            while e > 0 and len(done) <= items.index(("k", e)) + LAG:
+                step()
             take_q(e)
             take_k(e)
-            for h in range(hn):
-                head(group(e), h)
-                for s in range(1, p):
-                    a_copy(s, group(e), h).start()
-                step()
-        while len(done) < len(items) + LAG:
+        head(group(e), h)
+        for s in range(1, p):
+            a_copy(s, group(e), h).start()
+
+    def project(k):
+        while len(done) < min(len(items), items.index(("w", (k + 1) * sub - 1)) + 1) + LAG:
             step()
-    else:
-        while len(done) < len(items) + LAG:
-            step()
-        for e in range(m):
-            take_q(e)
-            take_k(e)
-
-        @pl.loop(0, m)
-        def _(e):
-            i = lax.rem(b + e, m)
-            for h in range(hn):
-                head(i, h)
-                for s in range(1, p):
-                    a_copy(s, i, h).start()
-
-    own_w.wait()
-    w_own.wait_recv()
-
-    for k in range(n):
+        if k == 0:
+            own_w.wait()
+            w_own.wait_recv()
         for u in range(k * sub, (k + 1) * sub):
             for o in range(1, nx):
                 for q in range(g):
@@ -402,15 +460,54 @@
             else:
                 out_ref[:, where] = (acc[:, where] + part_sum).astype(out_ref.dtype)
 
-    for o in range(1, n):
-        @pl.when(lat_sent(o))
+    own_k.wait()
+    work = [functools.partial(project, k) for k in range(n)]
+    if m * hn <= 2 * VARIANTS:
+        work = [functools.partial(attend, e, h) for e in range(m) for h in range(hn)] + work
+    else:
+        while len(done) < len(items) + LAG:
+            step()
+        for e in range(m):
+            take_q(e)
+            take_k(e)
+
+        @pl.loop(0, m)
+        def _(e):
+            i = lax.rem(b + e, m)
+            for h in range(hn):
+                head(i, h)
+                for s in range(1, p):
+                    a_copy(s, i, h).start()
+
+    for count in PLAN:
+        for _ in range(min(count, len(work))):
+            work.pop(0)()
+        step()
+    for piece in work:
+        piece()
+    while len(done) < len(items) + LAG:
+        step()
+
+    for s in range(1, p):
+        for copy in lat_mate(s):
+            copy.wait_send()
+    for o in range(1, m):
+        @pl.when(b + o < m)
         def _():
-            for copy in lat_copies(o):
+            for copy in lat_group(o):
                 copy.wait_send()
+
+        @pl.when(b - o >= 0)
+        def _():
+            for s in range(1, p):
+                for copy in lat_relay(o, s):
+                    copy.wait_send()
     for o in range(1, m):
-        kz_copy(o).wait_send()
+        for q in range(g):
+            kz_copy(o, q).wait_send()
     for e in range(m):
-        k_own(e).wait_send()
+        for q in range(g):
+            k_own(q, e).wait_send()
         for s in range(1, p):
             q_copy(s, e).wait_send()
             for h in range(hn):
@@ -421,7 +518,10 @@
         for o in range(1, nx):
             in_x(o, e).wait_send()
             for q in range(1, g):
-                in_y(o, q, e).wait_send()
+                if direct(kind, e):
+                    w_x(o, e, q).wait_send()
+                else:
+                    in_y(o, q, e).wait_send()
             for q in range(g):
                 in_c(o, q, e).wait_send()
 
@@ -453,7 +553,7 @@
     hbm = pl.BlockSpec(memory_space=pltpu.HBM)
     out = pl.pallas_call(
         functools.partial(kernel, n, g, nx, p, hn, rope, width**-0.5, sub),
-        out_shape=jax.ShapeDtypeStruct((tok, cols * dp), bf),
+        out_shape=pltpu.VMEM((tok, cols * dp), bf),
         in_specs=[hbm] * 7,
         out_specs=vmem,
         scratch_shapes=[
@@ -471,18 +571,20 @@
             pltpu.VMEM((1, latw), jnp.float32),
             pltpu.VMEM((2, rope // 2, p * tok), jnp.float32),
             dma((6 + m,)),
-            dma((n,)), dma((n,)), dma((n,)), dma((n,)),
+            dma((pn, 2)), dma((pn, 2)), dma((mn, 2)), dma((mn, 2)),
+            dma((mn, pn, 2)), dma((mn, pn, 2)),
             dma((pn, m)), dma((pn, m)),
-            dma((mn,)), dma((mn,)),
+            dma((mn, g)), dma((mn, g)),
             dma((pn, m, hn)), dma((pn, m, hn)),
             dma((xn, m)), dma((xn, m)),
             dma((xn, gn, m)), dma((xn, gn, m)),
             dma((xn, g, m)), dma((xn, g, m)),
-            dma((m,)), dma((m,)),
+            dma((g, m)), dma((g, m)),
             dma((xn, units)), dma((xn, units)),
             dma((xn, gn, units)), dma((xn, gn, units)),
             dma((xn, g, units)), dma((xn, g, units)),
             dma(()), dma(()),
+            pltpu.SemaphoreType.REGULAR,
         ],
         compiler_params=pltpu.CompilerParams(
             collective_id=0, has_side_effects=True, vmem_limit_bytes=60 * 1024 * 1024

time: 49.4 us -> 41.6 us (0.84)
  the two profiles are of different devices: /device:TPU:25 before, /device:TPU:0 now
where the time goes in v2:
time: 41.6 us; the launch traced here: 41.4 us
  Pallas kernels  40.6 us (98%)
  local copies, waits for them, and re-layouts  0.8 us (2%)
    pallas_call x1, Pallas kernels, body(): pl.pallas_call(functools.partial(kernel, n, g, nx, p, hn, rope, width **...  40.6 us

profile of v2, /device:TPU:0, one launch (start us, length us, event | category | flops | bytes accessed | tf_op | source)
XLA Modules:
  0.0 41.4 jit_solution(18242032578119398402)
XLA Ops:
  0.0 40.6 %shard_map.73 = bf16[128,2048]{1,0:T(8,128)(2,1)S(1)} custom-call(bf16[16,192,128]{2,1,0:T(8,128)(2,1)} %bitcast.10, bf16[128,512]{1,0:T(8,128)(2,1)} %bitcast.11, bf16[64,128]{1,0:T(8,128)(2,1)} %bitcast.12, f32[1,512]{1,0:T(1,128)} %bitcast.13, f32[2,32,512]{2,1,0:T(8,128)} %constant.2.clone.table_ref, bf16[128,1024]{1,0:T(8,128)(2,1)} %kvw_ref.1, ...), custom_call_target="tpu_custom_call" | custom-call | tf_op jit(solution)/shard_map/pallas_call | solution.py:554
  40.6 0.8 %copy.9 = bf16[1,128,2048]{2,1,0:T(8,128)(2,1)} copy(bf16[1,128,2048]{2,1,0:T(8,128)(2,1)S(1)} %bitcast.9) | data formatting | bytes 1048576

commit v3 on v2

--- a/solution.py
+++ b/solution.py
@@ -16,12 +16,18 @@
 UNITS = 16
 LEAD = 4
 LAG = 4
-KEYS = 7
-RELAY = 8
-LATE = 12
-START = 12
+KEYS = 8
+RELAY = 9
+LATE = 13
+START = 14
 DIRECT = 1
-PLAN = (1, 1, 1, 1, 2, 2, 1, 1, 1)
+PIECES = 2
+TILE = 16
+APART = 1
+EXTRA = 1
+HEADS = 2
+KEEP = 7
+PLAN = (1, 0, 1, 0, 1, 1, 1, 1, 1)
 SPLIT = 2
 VARIANTS = 4
 MESH = pl.DeviceIdType.MESH
@@ -39,7 +45,7 @@
     q_ref, latent_ref, key_ref, gain_ref, table_ref, kvw_ref, w_ref, out_ref,
     qbuf, lat, rkey, shared, kvw, wfull, attout, attin, acc, latin, keyin, gain, table,
     loc, lm_s, lm_r, lg_s, lg_r, lr_s, lr_r, q_s, q_r, kz_s, kz_r, a_s, a_r,
-    kx_s, kx_r, ky_s, ky_r, kc_s, kc_r, ko_s, ko_r,
+    kx_s, kx_r, kf_s, kf_r, ky_s, ky_r, kc_s, kc_r, ko_s, ko_r,
     wx_s, wx_r, wy_s, wy_r, wc_s, wc_r, wo_s, wo_r, far,
 ):
     me = lax.axis_index("sp")
@@ -54,6 +60,8 @@
     rrows = rkey.shape[1]
     krows = kvw_ref.shape[0]
     kh = krows // g
+    pieces = math.gcd(PIECES, max(1, kh // TILE))
+    ks = kh // pieces
     cols = w_ref.shape[1]
     kd = hn * VD
     part = kd // g
@@ -183,22 +191,36 @@
     def k_rows(i, d, q):
         return kvw.at[i, span(d * krows + q * kh, kh)]
 
-    def k_x(o, e):
-        dst = k_rows(group(e), dp, y)
-        src = kvw_ref.at[span(y * kh, kh)] if e == 0 else dst
+    def k_piece(i, d, q, f):
+        return kvw.at[i, pl.ds(pl.multiple_of(d * krows + q * kh + f * ks, TILE), ks)]
+
+    def k_x(o, ef):
+        e, f = ef
+        dst = k_piece(group(e), dp, y, f)
+        src = kvw_ref.at[pl.ds(pl.multiple_of(y * kh + f * ks, TILE), ks)] if e == 0 else dst
         return remote(
-            src, dst, kx_s.at[o - 1, e], kx_r.at[o - 1, e], chip(lax.rem(x + o, nx), c)
-        )
-
-    def k_y(o, q, e):
-        ref = k_rows(group(e), xs(o), y)
+            src, dst, kx_s.at[o - 1, e, f], kx_r.at[o - 1, e, f], chip(lax.rem(x + o, nx), c)
+        )
+
+    def k_down(s, o, f):
+        ref = k_piece(b, xs(o), y, f)
         return remote(
-            ref, ref, ky_s.at[o - 1, q - 1, e], ky_r.at[o - 1, q - 1, e], {"grp": lax.rem(y + q, g)}
-        )
-
-    def k_c(o, q, e):
-        ref = k_rows(group(e), xs(o), lax.rem(y + g - q, g))
-        return remote(ref, ref, kc_s.at[o - 1, q, e], kc_r.at[o - 1, q, e], partner)
+            ref, ref, kf_s.at[s - 1, o - 1, f], kf_r.at[s - 1, o - 1, f],
+            {"sp": lax.rem(b + m - s, m) * p + r},
+        )
+
+    def k_y(o, q, ef):
+        e, f = ef
+        ref = k_piece(group(e), xs(o), y, f)
+        return remote(
+            ref, ref, ky_s.at[o - 1, q - 1, e, f], ky_r.at[o - 1, q - 1, e, f],
+            {"grp": lax.rem(y + q, g)},
+        )
+
+    def k_c(o, q, ef):
+        e, f = ef
+        ref = k_piece(group(e), xs(o), lax.rem(y + g - q, g), f)
+        return remote(ref, ref, kc_s.at[o - 1, q, e, f], kc_r.at[o - 1, q, e, f], partner)
 
     def k_own(q, e):
         part_of = lax.rem(y + q, g)
@@ -221,6 +243,18 @@
 
     def direct(kind, u):
         return kind == "w" and u >= units - DIRECT
+
+    def maybe(kind, u):
+        return m > 1 and kind == "w" and units - DIRECT - EXTRA <= u < units - DIRECT
+
+    def crossing(kind, u, yes, no):
+        if direct(kind, u):
+            yes()
+        elif maybe(kind, u):
+            pl.when(b + 1 < m)(yes)
+            pl.when(b + 1 >= m)(no)
+        else:
+            no()
 
     def w_x(o, u, q=0):
         rows = w_rows(lax.rem(y + g - q, g), u)
@@ -242,57 +276,160 @@
     w_own = remote(w_ref, wfull.at[dp], wo_s, wo_r, partner)
 
     items = [("w", u) for u in range(units)]
-    for e in range(1, m):
-        items.insert(KEYS + (e - 1) * (units - KEYS) // (m - 1), ("k", e))
-    items.insert(1, ("k", 0))
+    for f in range(pieces):
+        for e in range(1, m):
+            where = KEYS + (e - 1) * (units - KEYS) // (m - 1)
+            items.insert(where + f * APART, ("k", (e, f)))
+    for f in range(pieces):
+        items.insert(1 + f, ("k", (0, f)))
 
     def issue(s):
         if s >= len(items):
             return
         kind, e = items[s]
         if kind == "k":
-            if e > 0:
+            e, f = e
+            if e > 0 and f == 0:
                 kz_copy(m - e, 0).wait_recv()
-            for o in range(1, nx):
-                k_x(o, e).start()
-            for q in range(g if e == 0 else 1):
-                k_own(q, e).start()
+
+            @pl.when((b + e >= m) | (e == 0))
+            def _():
+                for o in range(1, nx):
+                    k_x(o, (e, f)).start()
+
+            if f == 0:
+                for q in range(g if e == 0 else 1):
+                    k_own(q, e).start()
         else:
-            for o in range(1, nx):
-                for q in range(g if direct(kind, e) else 1):
-                    w_x(o, e, q).start()
+            def more():
+                for o in range(1, nx):
+                    for q in range(1, g):
+                        w_x(o, e, q).start()
+
+            for o in range(1, nx):
+                w_x(o, e).start()
+            crossing(kind, e, more, lambda: None)
 
     def pass_x(s):
         if s >= len(items):
             return
         kind, e = items[s]
-        for o in range(1, nx):
-            if direct(kind, e):
-                for q in range(g):
+        in_x, in_y, in_c = (k_x, k_y, k_c) if kind == "k" else (w_x, w_y, w_c)
+        if kind == "k" and e[0] > 0:
+            @pl.when(b + e[0] >= m)
+            def _():
+                for o in range(1, nx):
+                    k_x(o, e).wait_recv()
+
+            @pl.when(b + e[0] < m)
+            def _():
+                for o in range(1, nx):
+                    k_down(e[0], o, e[1]).wait_recv()
+        else:
+            for o in range(1, nx):
+                in_x(o, e).wait_recv()
+
+        def yes():
+            for o in range(1, nx):
+                in_c(o, 0, e).start()
+                for q in range(1, g):
                     w_x(o, e, q).wait_recv()
-                    w_c(o, q, e).start()
-                continue
-            in_x, in_y, in_c = (k_x, k_y, k_c) if kind == "k" else (w_x, w_y, w_c)
-            in_x(o, e).wait_recv()
-            for q in range(1, g):
-                in_y(o, q, e).start()
-            in_c(o, 0, e).start()
+                    in_c(o, q, e).start()
+
+        def no():
+            for o in range(1, nx):
+                for q in range(1, g):
+                    in_y(o, q, e).start()
+                in_c(o, 0, e).start()
+
+        crossing(kind, e, yes, no)
+        if kind == "k" and e[0] == 0:
+            for o in range(1, m):
+                @pl.when(b - o >= 0)
+                def _():
+                    for d in range(1, nx):
+                        k_down(o, d, e[1]).start()
 
     def pass_y(s):
-        if s < 0 or s >= len(items) or direct(*items[s]):
+        if s < 0 or s >= len(items):
             return
         kind, e = items[s]
         in_y, in_c = (k_y, k_c) if kind == "k" else (w_y, w_c)
+
+        def no():
+            for o in range(1, nx):
+                for q in range(1, g):
+                    in_y(o, q, e).wait_recv()
+                    in_c(o, q, e).start()
+
+        crossing(kind, e, lambda: None, no)
+
+    def settle():
+        for s in range(1, p):
+            for copy in lat_mate(s):
+                copy.wait_send()
+        for o in range(1, m):
+            @pl.when(b + o < m)
+            def _():
+                for copy in lat_group(o):
+                    copy.wait_send()
+
+            @pl.when(b - o >= 0)
+            def _():
+                for s in range(1, p):
+                    for copy in lat_relay(o, s):
+                        copy.wait_send()
+
+            for q in range(g):
+                kz_copy(o, q).wait_send()
+        for e in range(m):
+            for q in range(g):
+                k_own(q, e).wait_send()
+            for s in range(1, p):
+                q_copy(s, e).wait_send()
+        w_own.wait_send()
+
+    def retire(s):
+        if s < 0 or s >= len(items):
+            return
+        kind, e = items[s]
+        in_x, in_y, in_c = (k_x, k_y, k_c) if kind == "k" else (w_x, w_y, w_c)
+        if kind == "k" and e[0] > 0:
+            @pl.when(b + e[0] >= m)
+            def _():
+                for o in range(1, nx):
+                    k_x(o, e).wait_send()
+        else:
+            for o in range(1, nx):
+                in_x(o, e).wait_send()
+        if kind == "k" and e[0] == 0:
+            for o in range(1, m):
+                @pl.when(b - o >= 0)
+                def _():
+                    for d in range(1, nx):
+                        k_down(o, d, e[1]).wait_send()
+
+        def yes():
+            for o in range(1, nx):
+                for q in range(1, g):
+                    w_x(o, e, q).wait_send()
+
+        def no():
+            for o in range(1, nx):
+                for q in range(1, g):
+                    in_y(o, q, e).wait_send()
+
+        crossing(kind, e, yes, no)
         for o in range(1, nx):
-            for q in range(1, g):
-                in_y(o, q, e).wait_recv()
-                in_c(o, q, e).start()
+            for q in range(g):
+                in_c(o, q, e).wait_send()
 
     done = []
+    total = len(items) + LAG
 
     def step():
         s = len(done)
-        if s >= len(items) + LAG:
+        if s >= total:
             return
         done.append(s)
         if s == RELAY:
@@ -305,6 +442,7 @@
         issue(s + LEAD)
         pass_x(s)
         pass_y(s - LAG)
+        retire(s - KEEP)
 
     along = beside if staged else (p - 1) + (m - 1)
     pl.semaphore_wait(barrier, along + (nx - 1) + (g - 1) + 1)
@@ -403,11 +541,12 @@
         for t in range(p):
             attout[i, t, h] = o[:, t * tok : (t + 1) * tok].T.astype(jnp.bfloat16)
 
-    def head(i, h):
+    def head(i, start):
         for v in range(variants):
             @pl.when(lax.div(b, m // variants) == v)
             def _():
-                head_over(i, h, (v + 1) * stride)
+                for h in range(start, min(start + HEADS, hn)):
+                    head_over(i, h, (v + 1) * stride)
 
     def take_q(e):
         i = group(e)
@@ -420,17 +559,19 @@
             k_own(q, e).wait_recv()
         for o in range(1, nx):
             for q in range(g):
-                k_c(o, q, e).wait_recv()
+                for f in range(pieces):
+                    k_c(o, q, (e, f)).wait_recv()
 
     def attend(e, h):
         if h == 0:
-            while e > 0 and len(done) <= items.index(("k", e)) + LAG:
+            while e > 0 and len(done) <= items.index(("k", (e, pieces - 1))) + LAG:
                 step()
             take_q(e)
             take_k(e)
         head(group(e), h)
-        for s in range(1, p):
-            a_copy(s, group(e), h).start()
+        for k in range(h, min(h + HEADS, hn)):
+            for s in range(1, p):
+                a_copy(s, group(e), k).start()
 
     def project(k):
         while len(done) < min(len(items), items.index(("w", (k + 1) * sub - 1)) + 1) + LAG:
@@ -463,9 +604,9 @@
     own_k.wait()
     work = [functools.partial(project, k) for k in range(n)]
     if m * hn <= 2 * VARIANTS:
-        work = [functools.partial(attend, e, h) for e in range(m) for h in range(hn)] + work
+        work = [functools.partial(attend, e, h) for e in range(m) for h in range(0, hn, HEADS)] + work
     else:
-        while len(done) < len(items) + LAG:
+        while len(done) < total:
             step()
         for e in range(m):
             take_q(e)
@@ -474,8 +615,9 @@
         @pl.loop(0, m)
         def _(e):
             i = lax.rem(b + e, m)
+            for h in range(0, hn, HEADS):
+                head(i, h)
             for h in range(hn):
-                head(i, h)
                 for s in range(1, p):
                     a_copy(s, i, h).start()
 
@@ -483,47 +625,19 @@
         for _ in range(min(count, len(work))):
             work.pop(0)()
         step()
-    for piece in work:
+    for piece in work[:-1]:
         piece()
-    while len(done) < len(items) + LAG:
+    settle()
+    work[-1]()
+    while len(done) < total:
         step()
 
-    for s in range(1, p):
-        for copy in lat_mate(s):
-            copy.wait_send()
-    for o in range(1, m):
-        @pl.when(b + o < m)
-        def _():
-            for copy in lat_group(o):
-                copy.wait_send()
-
-        @pl.when(b - o >= 0)
-        def _():
-            for s in range(1, p):
-                for copy in lat_relay(o, s):
-                    copy.wait_send()
-    for o in range(1, m):
-        for q in range(g):
-            kz_copy(o, q).wait_send()
+    for s in range(total - KEEP, len(items)):
+        retire(s)
     for e in range(m):
-        for q in range(g):
-            k_own(q, e).wait_send()
         for s in range(1, p):
-            q_copy(s, e).wait_send()
             for h in range(hn):
                 a_copy(s, group(e), h).wait_send()
-    w_own.wait_send()
-    for kind, e in items:
-        in_x, in_y, in_c = (k_x, k_y, k_c) if kind == "k" else (w_x, w_y, w_c)
-        for o in range(1, nx):
-            in_x(o, e).wait_send()
-            for q in range(1, g):
-                if direct(kind, e):
-                    w_x(o, e, q).wait_send()
-                else:
-                    in_y(o, q, e).wait_send()
-            for q in range(g):
-                in_c(o, q, e).wait_send()
 
 
 def body(sizes, queries, kv_latent, rope_key, kv_gain, kv_weight, out_weight):
@@ -576,9 +690,10 @@
             dma((pn, m)), dma((pn, m)),
             dma((mn, g)), dma((mn, g)),
             dma((pn, m, hn)), dma((pn, m, hn)),
-            dma((xn, m)), dma((xn, m)),
-            dma((xn, gn, m)), dma((xn, gn, m)),
-            dma((xn, g, m)), dma((xn, g, m)),
+            dma((xn, m, PIECES)), dma((xn, m, PIECES)),
+            dma((mn, xn, PIECES)), dma((mn, xn, PIECES)),
+            dma((xn, gn, m, PIECES)), dma((xn, gn, m, PIECES)),
+            dma((xn, g, m, PIECES)), dma((xn, g, m, PIECES)),
             dma((g, m)), dma((g, m)),
             dma((xn, units)), dma((xn, units)),
             dma((xn, gn, units)), dma((xn, gn, units)),

time: 41.6 us -> 40.9 us (0.983); the launches traced: 41.4 us -> 40.2 us
  Pallas kernels: 40.6 us -> 39.4 us
    pallas_call x1, Pallas kernels: 40.6 us -> 39.4 us  [body(): pl.pallas_call(functools.partial(kernel, n, g, nx, p, hn, rope, width **...]
where the time goes in v3:
time: 40.9 us; the launch traced here: 40.2 us
  Pallas kernels  39.4 us (96%)
  local copies, waits for them, and re-layouts  0.8 us (2%)
    pallas_call x1, Pallas kernels, body(): pl.pallas_call(functools.partial(kernel, n, g, nx, p, hn, rope, width **...  39.4 us

profile of v3, /device:TPU:0, one launch (start us, length us, event | category | flops | bytes accessed | tf_op | source)
XLA Modules:
  0.0 40.2 jit_solution(2098053506306642091)
XLA Ops:
  0.0 39.4 %shard_map.73 = bf16[128,2048]{1,0:T(8,128)(2,1)S(1)} custom-call(bf16[16,192,128]{2,1,0:T(8,128)(2,1)} %bitcast.10, bf16[128,512]{1,0:T(8,128)(2,1)} %bitcast.11, bf16[64,128]{1,0:T(8,128)(2,1)} %bitcast.12, f32[1,512]{1,0:T(1,128)} %bitcast.13, f32[2,32,512]{2,1,0:T(8,128)} %constant.2.clone.table_ref, bf16[128,1024]{1,0:T(8,128)(2,1)} %kvw_ref.1, ...), custom_call_target="tpu_custom_call" | custom-call | tf_op jit(solution)/shard_map/pallas_call | solution.py:668
  39.4 0.8 %copy.9 = bf16[1,128,2048]{2,1,0:T(8,128)(2,1)} copy(bf16[1,128,2048]{2,1,0:T(8,128)(2,1)S(1)} %bitcast.9) | data formatting | bytes 1048576

commit v4 on v3

--- a/solution.py
+++ b/solution.py
@@ -27,7 +27,7 @@
 EXTRA = 1
 HEADS = 2
 KEEP = 7
-PLAN = (1, 0, 1, 0, 1, 1, 1, 1, 1)
+PLAN = (0, 1, 1, 0, 1, 1, 1, 1, 1)
 SPLIT = 2
 VARIANTS = 4
 MESH = pl.DeviceIdType.MESH
@@ -440,8 +440,8 @@
         if s == LATE:
             late()
         issue(s + LEAD)
+        pass_y(s - LAG)
         pass_x(s)
-        pass_y(s - LAG)
         retire(s - KEEP)
 
     along = beside if staged else (p - 1) + (m - 1)

time: 40.9 us -> 40.7 us (level)
  no operation moved by 1% of the time
where the time goes in v4:
time: 40.7 us; the launch traced here: 40.2 us
  Pallas kernels  39.4 us (97%)
  local copies, waits for them, and re-layouts  0.8 us (2%)
    pallas_call x1, Pallas kernels, body(): pl.pallas_call(functools.partial(kernel, n, g, nx, p, hn, rope, width **...  39.4 us

profile of v4, /device:TPU:0, one launch (start us, length us, event | category | flops | bytes accessed | tf_op | source)
XLA Modules:
  0.0 40.2 jit_solution(10490170129519486564)
XLA Ops:
  0.0 39.4 %shard_map.73 = bf16[128,2048]{1,0:T(8,128)(2,1)S(1)} custom-call(bf16[16,192,128]{2,1,0:T(8,128)(2,1)} %bitcast.10, bf16[128,512]{1,0:T(8,128)(2,1)} %bitcast.11, bf16[64,128]{1,0:T(8,128)(2,1)} %bitcast.12, f32[1,512]{1,0:T(1,128)} %bitcast.13, f32[2,32,512]{2,1,0:T(8,128)} %constant.2.clone.table_ref, bf16[128,1024]{1,0:T(8,128)(2,1)} %kvw_ref.1, ...), custom_call_target="tpu_custom_call" | custom-call | tf_op jit(solution)/shard_map/pallas_call | solution.py:668
  39.4 0.8 %copy.9 = bf16[1,128,2048]{2,1,0:T(8,128)(2,1)} copy(bf16[1,128,2048]{2,1,0:T(8,128)(2,1)S(1)} %bitcast.9) | data formatting | bytes 1048576
